TPU v7x, 32 devices: a whole 2x2x4 slice. The times are simulated.
32 devices in a mesh: fs: 4 (over z), rep: 4 (over y, x), tp: 2 (over core).
Axes of the slice: x: 2, y: 2, z: 4, core: 2. Of those that a mesh axis runs over, the one named last changes fastest.
Arguments:
- first_mix: bfloat16 [12288, 2048], P(('fs', 'rep'), 'tp'), may hold values from -6 to 6
- second_mix: bfloat16 [12288, 2048], P(('fs', 'rep'), 'tp'), may hold values from -6 to 6
- lambda_head: float32 [8], P('tp'), may hold values from 0.3 to 0.8
- head_gain: float32 [256], replicated, may hold values from 0.1 to 1.9
- out_cotangent: bfloat16 [12288, 2048], P(('fs', 'rep')), may hold values from -0.053955078 to 0.053955078
- basis: bfloat16 [2048, 256], P('tp'), may hold values from -0.125 to 0.125
- weight: float32 [2048, 2048], P('tp', 'fs'), may hold values from -3 to 3
- first_moment: float32 [2048, 256], P('fs', 'tp'), may hold values from -4.5 to 4.5
- second_moment: float32 [2048, 256], P('fs', 'tp'), may hold values from 0.05 to 0.5
Outputs:
- weight_new: float32 [2048, 2048], P('tp', 'fs')
- weight_copy: bfloat16 [2048, 2048], P('tp')
- step_out: float32 [2048, 2048], P('tp', 'fs')
- first_new: float32 [2048, 256], P('fs', 'tp')
- second_new: float32 [2048, 256], P('fs', 'tp')
All inputs are finite; a program needn't handle non-finite values.
Results may differ from a plain program's by a relative error of at most 0.0075.
Values may be sent and summed in bfloat16 or wider, within the bound.
A program may use at most 64 MiB of HBM per device.

v0:
```python
import jax
import jax.numpy as jnp
from jax import lax
from jax.sharding import PartitionSpec as P

out_scale = 0.8
beta_first = 0.9
beta_second = 0.95


def head_output(first_piece, second_piece, lambdas, head_gain):
    token_count = first_piece.shape[0]
    head_width = head_gain.shape[0]
    head_count = lambdas.shape[0] // head_width
    mixture = first_piece.astype(jnp.float32) - lambdas[None, :] * second_piece.astype(jnp.float32)
    grouped = mixture.reshape(token_count, head_count, head_width)
    inverse = lax.rsqrt(jnp.mean(grouped * grouped, axis=-1, keepdims=True) + 1e-06)
    normed = grouped * inverse * head_gain[None, None, :] * out_scale
    return normed.reshape(token_count, head_count * head_width).astype(jnp.bfloat16)


def split_product(narrow, wide, numbers):
    upper = wide.astype(jnp.bfloat16)
    lower = (wide - upper.astype(jnp.float32)).astype(jnp.bfloat16)
    return lax.dot_general(
        narrow, upper, numbers, preferred_element_type=jnp.float32
    ) + lax.dot_general(narrow, lower, numbers, preferred_element_type=jnp.float32)


def body(
    first_mix,
    second_mix,
    lambda_head,
    head_gain,
    out_cotangent,
    basis,
    weight,
    first_moment,
    second_moment,
):
    lambdas = jnp.repeat(lambda_head, head_gain.shape[0])
    head_out = head_output(first_mix, second_mix, lambdas, head_gain)
    reduced = jnp.dot(head_out, basis, preferred_element_type=jnp.float32)
    proj_rows = lax.psum_scatter(
        split_product(out_cotangent, reduced, (((0,), (0,)), ((), ()))),
        "fs",
        scatter_dimension=0,
        tiled=True,
    )
    proj_rows = lax.psum_scatter(proj_rows, "tp", scatter_dimension=1, tiled=True)
    projected = lax.psum(proj_rows, "rep")
    first_new = beta_first * first_moment + (1.0 - beta_first) * projected
    second_new = beta_second * second_moment + (1.0 - beta_second) * projected * projected
    direction = first_new / (jnp.sqrt(second_new) + 1e-08)
    energy = lax.psum(jnp.sum(direction * direction), ("fs", "tp"))
    entries = direction.shape[0] * direction.shape[1] * lax.axis_size("fs") * lax.axis_size("tp")
    spread = jnp.sqrt(energy / entries)
    full_direction = lax.all_gather(direction, "tp", axis=1, tiled=True)
    step_out = split_product(basis, full_direction, (((1,), (1,)), ((), ()))) * (
        -1.0 / (spread + 1e-06)
    )
    weight_new = weight + step_out
    weight_copy = lax.all_gather(weight_new.astype(jnp.bfloat16), "fs", axis=1, tiled=True)
    return (weight_new, weight_copy, step_out, first_new, second_new)


def solution(mesh):
    return jax.shard_map(
        body,
        mesh=mesh,
        in_specs=(
            P(("fs", "rep"), "tp"),
            P(("fs", "rep"), "tp"),
            P("tp"),
            P(),
            P(("fs", "rep"), None),
            P("tp", None),
            P("tp", "fs"),
            P("fs", "tp"),
            P("fs", "tp"),
        ),
        out_specs=(P("tp", "fs"), P("tp", None), P("tp", "fs"), P("fs", "tp"), P("fs", "tp")),
        check_vma=False,
    )
```

profile of v0, /device:TPU:0, one launch (start us, length us, event | category | flops | bytes accessed | tf_op | source)
XLA Modules:
  0.0 254.0 jit_solution(11689265764747644795)
XLA Ops:
  7.2 0.0 copy-start
  7.2 0.0 reduce-scatter.3.cloned.1.call-start
  7.2 0.9 broadcast_bitcast_fusion.1
  8.1 0.7 broadcast_bitcast_fusion
  8.8 4.2 %fusion = f32[768,1024]{1,0:T(8,128)} fusion(bf16[768,1024]{1,0:T(8,128)(2,1)} %param.10, bf16[768,1024]{1,0:T(8,128)(2,1)} %param.9, f32[1024]{0:T(1024)S(1)} %bitcast.19), kind=kLoop, calls=%fused_computation.2 | loop fusion | flops 3932160 | bytes 6295552 | tf_op jit(solution)/shard_map/mul | solution.py:17
  13.0 5.2 %mul.92 = f32[768,4,256]{2,1,0:T(4,128)} reshape(f32[768,1024]{1,0:T(8,128)} %fusion) | data formatting | bytes 6291456 | tf_op jit(solution)/shard_map/mul | solution.py:17
  18.2 2.8 %reduce_sum.18 = f32[768,4]{1,0:T(8,128)S(1)} reduce(f32[768,4,256]{2,1,0:T(4,128)} %mul.92, f32[]{:T(128)} %constant.2.clone.1), dimensions={2}, to_apply=%region_0.0 | reduce | flops 783360 | bytes 3158020 | tf_op jit(solution)/shard_map/reduce_sum | solution.py:17
  21.0 0.1 add_rsqrt_fusion
  21.1 1.0 mul.93
  22.0 0.0 copy-start.1
  22.1 0.0 copy-start.2
  22.1 0.0 copy-start.3
  22.1 0.8 copy.42
  22.8 0.6 copy-done.1
  23.5 0.5 copy-done.2
  23.9 0.1 copy-done.3
  24.0 0.9 fusion.2
  25.0 0.0 copy-done
  25.0 1.0 fusion.5
  26.0 0.0 copy-start.6
  26.0 2.4 fusion.1
  28.4 0.0 reduce-scatter.3.cloned.1.call-update
  28.4 0.0 reduce-scatter.5.cloned.1.call-start
  28.5 46.5 %reduce-scatter.3.cloned.1.call-done = f32[512,256]{0,1:T(8,128)} async-done(((f32[2048,256]{0,1:T(8,128)}), f32[512,256]{0,1:T(8,128)}) %reduce-scatter.3.cloned.1.call-update) | async-done | bytes 524304 | tf_op jit(solution)/shard_map/reduce_scatter | solution.py:44
  74.9 0.0 reduce-scatter.5.cloned.1.call-update
  74.9 0.0 all-reduce.2.cloned.1.call-start
  75.0 9.3 %reduce-scatter.5.cloned.1.call-done = f32[512,128]{0,1:T(8,128)} async-done(((f32[512,256]{0,1:T(8,128)}), f32[512,128]{0,1:T(8,128)}) %reduce-scatter.5.cloned.1.call-update) | async-done | bytes 262160 | tf_op jit(solution)/shard_map/reduce_scatter | solution.py:50
  84.3 0.0 all-reduce.2.cloned.1.call-update
  84.4 0.0 all-gather.2.cloned.1.call-start
  84.4 0.0 copy-done.6
  84.4 0.8 copy.31
  85.2 1.8 copy.34
  87.0 2.9 %copy.35 = f32[1024,512]{0,1:T(8,128)} copy(f32[1024,512]{1,0:T(8,128)} %param.15) | data formatting | bytes 4194304 | tf_op args[6]
  89.9 41.6 %all-reduce.2.cloned.1.call-done = f32[512,128]{0,1:T(8,128)} async-done(((f32[512,128]{0,1:T(8,128)}), f32[512,128]{0,1:T(8,128)}) %all-reduce.2.cloned.1.call-update) | async-done | bytes 262160 | tf_op jit(solution)/shard_map/psum | solution.py:51
  131.5 2.6 %multiply_reduce_fusion = (f32[]{:T(128)}, f32[512,128]{0,1:T(8,128)S(1)}, f32[512,128]{0,1:T(8,128)}, f32[512,128]{0,1:T(8,128)}) fusion(f32[512,128]{0,1:T(8,128)} %all-reduce.2.cloned.1.call-done, f32[512,128]{0,1:T(8,128)} %copy.34, f32[512,128]{0,1:T(8,128)} %copy.31), kind=kLoop, calls=%fused_computation.12 | loop fusion | flops 720895 | bytes 1572868 | tf_op jit(solution)/shard_map/reduce_sum | solution.py:55
  134.1 16.5 %psum.15 = f32[]{:T(128)} all-reduce(f32[]{:T(128)} %get-tuple-element.22), channel_id=1, replica_groups=mesh['fs'=4,'rep'=4,'tp'=2] {'fs','tp'}, use_global_device_ids=true, to_apply=%region_5.0 | all-reduce | flops 1 | bytes 8 | tf_op jit(solution)/shard_map/psum | solution.py:55
  151.3 2.2 all_gather.6
  153.5 0.0 copy-start.4
  153.5 0.8 copy-done.4
  154.3 2.8 %fusion.8 = f32[512,1024]{1,0:T(8,128)} fusion(bf16[1024,256]{1,0:T(8,128)(2,1)} %param.14, f32[512,256]{0,1:T(8,128)S(1)} %all_gather.6), kind=kOutput, calls=%fused_computation.19 | convolution fusion | flops 268566528 | bytes 3145728 | tf_op jit(solution)/shard_map/dot_general | solution.py:25
  157.2 0.0 copy-start.5
  157.2 5.7 %fusion.11 = (bf16[1024,512]{0,1:T(8,128)(2,1)}, f32[1024,512]{0,1:T(8,128)}, f32[1024,512]{0,1:T(8,128)}) fusion(f32[1024,512]{0,1:T(8,128)} %copy.35, f32[]{:T(128)S(6)} %div.19, f32[512,1024]{1,0:T(8,128)} %fusion.8, bf16[1024,256]{1,0:T(8,128)(2,1)} %param.14, f32[512,256]{0,1:T(8,128)} %copy-done.4), kind=kOutput, calls=%fused_computation.24 | convolution fusion | flops 271056896 | bytes 10485764 | tf_op jit(solution)/shard_map/dot_general | solution.py:27
  162.9 0.0 all-gather.2.cloned.1.call-update
  162.9 1.8 copy.40
  164.7 0.0 copy-done.5
  164.7 0.8 copy.39
  165.5 3.0 %copy.36 = f32[1024,512]{1,0:T(8,128)} copy(f32[1024,512]{0,1:T(8,128)} %get-tuple-element.21) | data formatting | bytes 4194304
  168.5 3.0 %copy.38 = f32[1024,512]{1,0:T(8,128)} copy(f32[1024,512]{0,1:T(8,128)} %get-tuple-element.26) | data formatting | bytes 4194304
  171.5 69.5 %all-gather.2.cloned.1.call-done = bf16[1024,2048]{0,1:T(8,128)(2,1)} async-done(((bf16[1024,512]{0,1:T(8,128)(2,1)}), bf16[1024,2048]{0,1:T(8,128)(2,1)}) %all-gather.2.cloned.1.call-update) | async-done | bytes 4194320 | tf_op jit(solution)/shard_map/all_gather | solution.py:63
  241.0 6.4 %copy.37 = bf16[1024,2048]{1,0:T(8,128)(2,1)} copy(bf16[1024,2048]{0,1:T(8,128)(2,1)} %all-gather.2.cloned.1.call-done) | data formatting | bytes 8388608
  (2 shorter events, 0.0 us)
Async XLA Ops:
  7.2 17.8 %copy-start = (bf16[768,2048]{1,0:T(8,128)(2,1)S(1)}, bf16[768,2048]{1,0:T(8,128)(2,1)}, u32[]{:S(2)}) copy-start(bf16[768,2048]{1,0:T(8,128)(2,1)} %param.13) | copy-start | bytes 9437188
  7.2 67.7 %reduce-scatter.3.cloned.1.call-start = ((), (), s32[]{:S(2)}) async-start(), calls=%async_computation.2 | async-start | bytes 2621440 | tf_op jit(solution)/shard_map/reduce_scatter | solution.py:44
  22.0 1.4 copy-start.1
  22.1 1.9 copy-start.2
  22.1 2.0 copy-start.3
  26.0 58.4 %copy-start.6 = (f32[512,128]{1,0:T(8,128)S(1)}, f32[512,128]{1,0:T(8,128)}, u32[]{:S(2)}) copy-start(f32[512,128]{1,0:T(8,128)} %param.16) | copy-start | bytes 786436
  28.4 55.9 %reduce-scatter.5.cloned.1.call-start = ((), (), s32[]{:S(2)}) async-start(), calls=%async_computation.3 | async-start | bytes 786432 | tf_op jit(solution)/shard_map/reduce_scatter | solution.py:50
  74.9 56.5 %all-reduce.2.cloned.1.call-start = ((), (), s32[]{:S(2)}) async-start(), calls=%async_computation.4 | async-start | bytes 524288 | tf_op jit(solution)/shard_map/psum | solution.py:51
  84.4 156.6 %all-gather.2.cloned.1.call-start = ((), (), s32[]{:S(2)}) async-start(), calls=%async_computation.5 | async-start | bytes 5242880 | tf_op jit(solution)/shard_map/all_gather | solution.py:63
  153.5 0.8 copy-start.4
  157.2 7.5 %copy-start.5 = (f32[512,128]{0,1:T(8,128)S(1)}, f32[512,128]{0,1:T(8,128)}, u32[]{:S(2)}) copy-start(f32[512,128]{0,1:T(8,128)} %get-tuple-element.25) | copy-start | bytes 786436
Sparse Core Ops, SparseCore 0:
  28.5 46.3 reduce-scatter.2
  77.2 7.1 reduce-scatter.4
  87.3 44.1 all-reduce.1
  163.0 77.9 all-gather.1
where the time goes:
time: 255 us; the launch traced here: 254 us
  waiting for transfers between devices  167 us (65%)
  local copies, waits for them, and re-layouts  31 us (12%)
  blocking collectives  18.7 us (7%)
  between operations  14.6 us (6%)
  matrix products  12.8 us (5%)
  other arithmetic  9.72 us (4%)
    all_gather x1, waiting for transfers between devices, body(): lax.all_gather(weight_new.astype(jnp.bfloat16), 'fs', axis=1, tiled=True)  69.5 us
    reduce_scatter x1, waiting for transfers between devices, body(): lax.psum_scatter(split_product(out_cotangent, reduced, (((0,), (0,)), (()...  46.5 us
    psum x1, waiting for transfers between devices, body(): projected = lax.psum(proj_rows, 'rep')  41.6 us
    unnamed x27, local copies, waits for them, and re-layouts  24.9 us
    psum x1, blocking collectives, body(): energy = lax.psum(jnp.sum(direction * direction), ('fs', 'tp'))  16.5 us
    reduce_scatter x1, waiting for transfers between devices, body(): lax.psum_scatter(proj_rows, 'tp', scatter_dimension=1, tiled=True)  9.34 us
    dot_general x2, matrix products, split_product(): lax.dot_general(narrow, lower, numbers, preferred_element_type=jnp.float32)  8.03 us
    mul x1, local copies, waits for them, and re-layouts, head_output(): grouped * grouped  5.15 us
  transfers between devices with their start and end apart: 4, of which 4 were waited for; matrix products, arithmetic and copies ran while one was open for 6% of the time, Pallas kernels for 0%

commit v1 on v0

--- a/solution.py
+++ b/solution.py
@@ -48,7 +48,7 @@
         tiled=True,
     )
     proj_rows = lax.psum_scatter(proj_rows, "tp", scatter_dimension=1, tiled=True)
-    projected = lax.psum(proj_rows, "rep")
+    projected = jnp.sum(lax.all_gather(proj_rows, "rep"), axis=0)
     first_new = beta_first * first_moment + (1.0 - beta_first) * projected
     second_new = beta_second * second_moment + (1.0 - beta_second) * projected * projected
     direction = first_new / (jnp.sqrt(second_new) + 1e-08)

time: 255 us -> 243 us (0.953)
  waiting for transfers between devices: 167 us -> 149 us
  local copies, waits for them, and re-layouts: 31 us -> 33.9 us
  other arithmetic: 9.72 us -> 12.3 us
    psum x1 -> x0, waiting for transfers between devices: 41.6 us -> none  [body(): projected = lax.psum(proj_rows, 'rep')]
    all_gather x0 -> x1, waiting for transfers between devices: none -> 23.9 us  [body(): projected = jnp.sum(lax.all_gather(proj_rows, 'rep'), axis=0)]
    all_gather x0 -> x1, local copies, waits for them, and re-layouts: none -> 2.9 us  [body(): projected = jnp.sum(lax.all_gather(proj_rows, 'rep'), axis=0)]
where the time goes in v1:
time: 243 us; the launch traced here: 242 us
  waiting for transfers between devices  149 us (61%)
  local copies, waits for them, and re-layouts  33.9 us (14%)
  blocking collectives  19 us (8%)
  between operations  14.6 us (6%)
  matrix products  12.8 us (5%)
  other arithmetic  12.3 us (5%)
    all_gather x1, waiting for transfers between devices, body(): lax.all_gather(weight_new.astype(jnp.bfloat16), 'fs', axis=1, tiled=True)  69.5 us
    reduce_scatter x1, waiting for transfers between devices, body(): lax.psum_scatter(split_product(out_cotangent, reduced, (((0,), (0,)), (()...  46.5 us
    unnamed x27, local copies, waits for them, and re-layouts  24.9 us
    all_gather x1, waiting for transfers between devices, body(): projected = jnp.sum(lax.all_gather(proj_rows, 'rep'), axis=0)  23.9 us
    psum x1, blocking collectives, body(): energy = lax.psum(jnp.sum(direction * direction), ('fs', 'tp'))  16.8 us
    reduce_scatter x1, waiting for transfers between devices, body(): lax.psum_scatter(proj_rows, 'tp', scatter_dimension=1, tiled=True)  9.34 us
    dot_general x2, matrix products, split_product(): lax.dot_general(narrow, lower, numbers, preferred_element_type=jnp.float32)  8.03 us
    mul x1, local copies, waits for them, and re-layouts, head_output(): grouped * grouped  5.15 us
  transfers between devices with their start and end apart: 4, of which 4 were waited for; matrix products, arithmetic and copies ran while one was open for 6% of the time, Pallas kernels for 0%

profile of v1, /device:TPU:0, one launch (start us, length us, event | category | flops | bytes accessed | tf_op | source)
XLA Modules:
  0.0 242.1 jit_solution(2006806133440303402)
XLA Ops:
  7.2 0.0 copy-start
  7.2 0.0 reduce-scatter.3.cloned.1.call-start
  7.2 0.9 broadcast_bitcast_fusion.1
  8.1 0.7 broadcast_bitcast_fusion
  8.8 4.2 %fusion = f32[768,1024]{1,0:T(8,128)} fusion(bf16[768,1024]{1,0:T(8,128)(2,1)} %param.10, bf16[768,1024]{1,0:T(8,128)(2,1)} %param.9, f32[1024]{0:T(1024)S(1)} %bitcast.21), kind=kLoop, calls=%fused_computation.2 | loop fusion | flops 3932160 | bytes 6295552 | tf_op jit(solution)/shard_map/mul | solution.py:17
  13.0 5.2 %mul.92 = f32[768,4,256]{2,1,0:T(4,128)} reshape(f32[768,1024]{1,0:T(8,128)} %fusion) | data formatting | bytes 6291456 | tf_op jit(solution)/shard_map/mul | solution.py:17
  18.2 2.8 %reduce_sum.27 = f32[768,4]{1,0:T(8,128)S(1)} reduce(f32[768,4,256]{2,1,0:T(4,128)} %mul.92, f32[]{:T(128)} %constant.2.clone.1), dimensions={2}, to_apply=%region_0.0 | reduce | flops 783360 | bytes 3158020 | tf_op jit(solution)/shard_map/reduce_sum | solution.py:17
  21.0 0.1 add_rsqrt_fusion
  21.1 1.0 mul.93
  22.0 0.0 copy-start.1
  22.1 0.0 copy-start.2
  22.1 0.0 copy-start.3
  22.1 0.8 copy.46
  22.8 0.6 copy-done.1
  23.5 0.5 copy-done.2
  23.9 0.1 copy-done.3
  24.0 0.9 fusion.2
  25.0 0.0 copy-done
  25.0 1.0 fusion.5
  26.0 0.0 copy-start.6
  26.0 2.4 fusion.1
  28.4 0.0 reduce-scatter.3.cloned.1.call-update
  28.4 0.0 reduce-scatter.5.cloned.1.call-start
  28.5 46.5 %reduce-scatter.3.cloned.1.call-done = f32[512,256]{0,1:T(8,128)} async-done(((f32[2048,256]{0,1:T(8,128)}), f32[512,256]{0,1:T(8,128)}) %reduce-scatter.3.cloned.1.call-update) | async-done | bytes 524304 | tf_op jit(solution)/shard_map/reduce_scatter | solution.py:44
  74.9 0.0 reduce-scatter.5.cloned.1.call-update
  74.9 0.0 all-gather.6.cloned.1.call-start
  75.0 9.3 %reduce-scatter.5.cloned.1.call-done = f32[512,128]{0,1:T(8,128)} async-done(((f32[512,256]{0,1:T(8,128)}), f32[512,128]{0,1:T(8,128)}) %reduce-scatter.5.cloned.1.call-update) | async-done | bytes 262160 | tf_op jit(solution)/shard_map/reduce_scatter | solution.py:50
  84.3 0.0 all-gather.6.cloned.1.call-update
  84.4 0.0 all-gather.4.cloned.1.call-start
  84.4 0.0 copy-done.6
  84.4 0.8 copy.35
  85.2 1.8 copy.38
  87.0 2.9 %copy.39 = f32[1024,512]{0,1:T(8,128)} copy(f32[1024,512]{1,0:T(8,128)} %param.15) | data formatting | bytes 4194304 | tf_op args[6]
  89.9 23.9 %all-gather.6.cloned.1.call-done = f32[2048,128]{0,1:T(8,128)} async-done(((f32[512,128]{0,1:T(8,128)}), f32[2048,128]{0,1:T(8,128)}) %all-gather.6.cloned.1.call-update) | async-done | bytes 1048592 | tf_op jit(solution)/shard_map/all_gather | solution.py:51
  113.8 2.9 %reshape.25 = f32[4,512,128]{1,0,2:T(4,128)} reshape(f32[2048,128]{0,1:T(8,128)} %all-gather.6.cloned.1.call-done) | data formatting | bytes 2097152 | tf_op jit(solution)/shard_map/all_gather | solution.py:51
  116.7 2.5 %reduce_sum.28 = f32[512,128]{0,1:T(8,128)} reduce(f32[4,512,128]{1,0,2:T(4,128)} %reshape.25, f32[]{:T(128)} %constant.2.clone.1), dimensions={0}, to_apply=%region_3.0 | reduce | flops 196608 | bytes 1310724 | tf_op jit(solution)/shard_map/reduce_sum | solution.py:51
  119.3 2.6 %multiply_reduce_fusion = (f32[]{:T(128)}, f32[512,128]{0,1:T(8,128)S(1)}, f32[512,128]{0,1:T(8,128)}, f32[512,128]{0,1:T(8,128)}) fusion(f32[512,128]{0,1:T(8,128)} %reduce_sum.28, f32[512,128]{0,1:T(8,128)} %copy.38, f32[512,128]{0,1:T(8,128)} %copy.35), kind=kLoop, calls=%fused_computation.12 | loop fusion | flops 720895 | bytes 1572868 | tf_op jit(solution)/shard_map/reduce_sum | solution.py:55
  121.9 16.8 %psum.7 = f32[]{:T(128)} all-reduce(f32[]{:T(128)} %get-tuple-element.27), channel_id=1, replica_groups=mesh['fs'=4,'rep'=4,'tp'=2] {'fs','tp'}, use_global_device_ids=true, to_apply=%region_5.0 | all-reduce | flops 1 | bytes 8 | tf_op jit(solution)/shard_map/psum | solution.py:55
  139.4 2.2 all_gather.14
  141.6 0.0 copy-start.4
  141.6 0.8 copy-done.4
  142.4 2.9 %fusion.8 = f32[512,1024]{1,0:T(8,128)} fusion(bf16[1024,256]{1,0:T(8,128)(2,1)} %param.14, f32[512,256]{0,1:T(8,128)S(1)} %all_gather.14), kind=kOutput, calls=%fused_computation.19 | convolution fusion | flops 268566528 | bytes 3145728 | tf_op jit(solution)/shard_map/dot_general | solution.py:25
  145.3 0.0 copy-start.5
  145.3 5.7 %fusion.11 = (bf16[1024,512]{0,1:T(8,128)(2,1)}, f32[1024,512]{0,1:T(8,128)}, f32[1024,512]{0,1:T(8,128)}) fusion(f32[1024,512]{0,1:T(8,128)} %copy.39, f32[]{:T(128)S(6)} %div.19, f32[512,1024]{1,0:T(8,128)} %fusion.8, bf16[1024,256]{1,0:T(8,128)(2,1)} %param.14, f32[512,256]{0,1:T(8,128)} %copy-done.4), kind=kOutput, calls=%fused_computation.24 | convolution fusion | flops 271056896 | bytes 10485764 | tf_op jit(solution)/shard_map/dot_general | solution.py:27
  151.0 0.0 all-gather.4.cloned.1.call-update
  151.0 1.8 copy.44
  152.8 0.0 copy-done.5
  152.8 0.8 copy.43
  153.6 3.0 %copy.40 = f32[1024,512]{1,0:T(8,128)} copy(f32[1024,512]{0,1:T(8,128)} %get-tuple-element.26) | data formatting | bytes 4194304
  156.6 2.9 %copy.42 = f32[1024,512]{1,0:T(8,128)} copy(f32[1024,512]{0,1:T(8,128)} %get-tuple-element.31) | data formatting | bytes 4194304
  159.6 69.5 %all-gather.4.cloned.1.call-done = bf16[1024,2048]{0,1:T(8,128)(2,1)} async-done(((bf16[1024,512]{0,1:T(8,128)(2,1)}), bf16[1024,2048]{0,1:T(8,128)(2,1)}) %all-gather.4.cloned.1.call-update) | async-done | bytes 4194320 | tf_op jit(solution)/shard_map/all_gather | solution.py:63
  229.1 6.4 %copy.41 = bf16[1024,2048]{1,0:T(8,128)(2,1)} copy(bf16[1024,2048]{0,1:T(8,128)(2,1)} %all-gather.4.cloned.1.call-done) | data formatting | bytes 8388608
  (2 shorter events, 0.0 us)
Async XLA Ops:
  7.2 17.8 %copy-start = (bf16[768,2048]{1,0:T(8,128)(2,1)S(1)}, bf16[768,2048]{1,0:T(8,128)(2,1)}, u32[]{:S(2)}) copy-start(bf16[768,2048]{1,0:T(8,128)(2,1)} %param.13) | copy-start | bytes 9437188
  7.2 67.7 %reduce-scatter.3.cloned.1.call-start = ((), (), s32[]{:S(2)}) async-start(), calls=%async_computation.2 | async-start | bytes 2621440 | tf_op jit(solution)/shard_map/reduce_scatter | solution.py:44
  22.0 1.4 copy-start.1
  22.1 1.9 copy-start.2
  22.1 2.0 copy-start.3
  26.0 58.4 %copy-start.6 = (f32[512,128]{1,0:T(8,128)S(1)}, f32[512,128]{1,0:T(8,128)}, u32[]{:S(2)}) copy-start(f32[512,128]{1,0:T(8,128)} %param.16) | copy-start | bytes 786436
  28.4 55.9 %reduce-scatter.5.cloned.1.call-start = ((), (), s32[]{:S(2)}) async-start(), calls=%async_computation.3 | async-start | bytes 786432 | tf_op jit(solution)/shard_map/reduce_scatter | solution.py:50
  74.9 38.9 %all-gather.6.cloned.1.call-start = ((), (), s32[]{:S(2)}) async-start(), calls=%async_computation.5 | async-start | bytes 1310720 | tf_op jit(solution)/shard_map/all_gather | solution.py:51
  84.4 144.8 %all-gather.4.cloned.1.call-start = ((), (), s32[]{:S(2)}) async-start(), calls=%async_computation.4 | async-start | bytes 5242880 | tf_op jit(solution)/shard_map/all_gather | solution.py:63
  141.6 0.8 copy-start.4
  145.3 7.5 %copy-start.5 = (f32[512,128]{0,1:T(8,128)S(1)}, f32[512,128]{0,1:T(8,128)}, u32[]{:S(2)}) copy-start(f32[512,128]{0,1:T(8,128)} %get-tuple-element.30) | copy-start | bytes 786436
Sparse Core Ops, SparseCore 0:
  28.5 46.3 reduce-scatter.2
  77.2 7.1 reduce-scatter.4
  86.2 27.6 all-gather.5
  151.1 77.9 all-gather.3
